TPU v7x, 32 devices: a whole 2x2x4 slice. The times are simulated.
32 devices in a mesh: kv: 4 (over y, x), tp: 8 (over z, core).
Axes of the slice: x: 2, y: 2, z: 4, core: 2. Of those that a mesh axis runs over, the one named last changes fastest.
Arguments:
- stream: bfloat16 [32, 4096], P(None, ('kv', 'tp')), may hold values from -18 to 18
- mixer_gain: float32 [4096], replicated, may hold values from 0.1 to 1.9
- query_weight: bfloat16 [4096, 1024], P(None, 'tp'), may hold values from -0.09375 to 0.09375
- key_weight: bfloat16 [4096, 1024], P(None, 'tp'), may hold values from -0.09375 to 0.09375
- value_weight: bfloat16 [4096, 1024], P(None, 'tp'), may hold values from -0.09375 to 0.09375
- forget_weight: bfloat16 [4096, 16], replicated, may hold values from -0.09375 to 0.09375
- forget_bias: float32 [16], replicated, may hold values from -4 to -2
- key_cache: bfloat16 [32, 16, 4096, 64], P(None, 'tp', 'kv'), may hold values from -512 to 512, as said below
- value_cache: bfloat16 [32, 16, 4096, 64], P(None, 'tp', 'kv'), may hold values from -12 to 12
- past_decay: float32 [32, 16, 4096], P(None, 'tp', 'kv'), may hold values from -4096 to 0, as said below
- out_weight: bfloat16 [1024, 4096], P('tp', 'kv'), may hold values from -0.75 to 0.75
- channel_gain: float32 [4096], replicated, may hold values from 0.1 to 1.9
- up_weight: bfloat16 [4096, 16384], P('kv', 'tp'), may hold values from -0.09375 to 0.09375
- down_weight: bfloat16 [16384, 4096], P('tp', 'kv'), may hold values from -0.0625 to 0.0625
Outputs:
- updated: bfloat16 [32, 4096], P(None, ('kv', 'tp'))
Inputs may be any that keep to these rules, and one draw needn't show every extreme that they name: `key_cache`: keys of order one; some cached keys may be much larger. `past_decay`: never falling along the positions of a sequence and head, zero at the last cached position.
All inputs are finite; a program needn't handle non-finite values.
Results may differ from a plain program's by a relative error of at most 0.014.
The roundings to bfloat16 on the way count: a program that leaves them out, or rounds other values in their place, can miss the bound.
Values may be sent and summed in bfloat16 or wider, within the bound.
No kernel may reach another device: no remote copies, remote signals or barrier semaphores. Data moves between devices by JAX's collectives and lax.ppermute only.
A program may use at most 64 MiB of HBM per device.

v0:
```python
import jax
import jax.numpy as jnp
from jax import lax
from jax.sharding import PartitionSpec as P

D = 4096
EPS = 1e-06


def combined_all(part, axis, combine):
    gathered = jax.tree.map(lambda a: lax.all_gather(a, axis), part)

    def take(source):
        return jax.tree.map(lambda a: lax.dynamic_index_in_dim(a, source, 0, False), gathered)

    return lax.fori_loop(
        1, lax.axis_size(axis), lambda source, state: combine(state, take(source)), take(0)
    )


def rms_scale(values, gain):
    widened = values.astype(jnp.float32)
    inverse = lax.rsqrt(jnp.mean(widened * widened, axis=-1, keepdims=True) + EPS)
    return (widened * inverse * gain).astype(jnp.bfloat16)


def merge_parts(earlier, later):
    top_one, total_one, sums_one = earlier
    top_two, total_two, sums_two = later
    highest = jnp.maximum(top_one, top_two)
    factor_one = jnp.exp(top_one - highest)
    factor_two = jnp.exp(top_two - highest)
    return (
        highest,
        total_one * factor_one + total_two * factor_two,
        sums_one * factor_one[..., None] + sums_two * factor_two[..., None],
    )


def squared_relu(values):
    return jnp.square(jax.nn.relu(values)).astype(jnp.bfloat16)


def row_squares(values):
    widened = values.astype(jnp.float32)
    return jnp.sum(widened * widened, axis=1)


def shards(
    stream,
    mixer_gain,
    query_weight,
    key_weight,
    value_weight,
    forget_weight,
    forget_bias,
    key_cache,
    value_cache,
    past_decay,
    out_weight,
    channel_gain,
    up_weight,
    down_weight,
):
    batch_rows = stream.shape[0]
    local_heads = key_cache.shape[1]
    head_size = key_cache.shape[3]
    scale_factor = float(head_size) ** (-0.5)
    gathered = lax.all_gather(stream, ("kv", "tp"), axis=1, tiled=True)
    normed = rms_scale(gathered, mixer_gain)
    queries = jnp.dot(normed, query_weight, preferred_element_type=jnp.float32).astype(jnp.bfloat16)
    keys_new = jnp.dot(normed, key_weight, preferred_element_type=jnp.float32).astype(jnp.bfloat16)
    values_new = jnp.dot(normed, value_weight, preferred_element_type=jnp.float32).astype(
        jnp.bfloat16
    )
    forget_all = jax.nn.log_sigmoid(
        jnp.dot(normed, forget_weight, preferred_element_type=jnp.float32) + forget_bias
    )
    forget = lax.dynamic_slice_in_dim(
        forget_all, lax.axis_index("tp") * local_heads, local_heads, 1
    )
    query_heads = queries.reshape(batch_rows, local_heads, head_size)
    scores = (
        jnp.einsum("bhd,bhpd->bhp", query_heads, key_cache, preferred_element_type=jnp.float32)
        * scale_factor
        + forget[..., None]
        + past_decay
    )
    highest = jnp.max(scores, axis=-1)
    weights = jnp.exp(scores - highest[..., None]).astype(jnp.bfloat16)
    totals = jnp.sum(weights.astype(jnp.float32), axis=-1)
    sums = jnp.einsum("bhp,bhpd->bhd", weights, value_cache, preferred_element_type=jnp.float32)
    highest, totals, sums = combined_all((highest, totals, sums), "kv", merge_parts)
    key_heads = keys_new.reshape(batch_rows, local_heads, head_size).astype(jnp.float32)
    value_heads = values_new.reshape(batch_rows, local_heads, head_size).astype(jnp.float32)
    own = jnp.sum(query_heads.astype(jnp.float32) * key_heads, axis=-1) * scale_factor
    peak = jnp.maximum(highest, own)
    cache_factor = jnp.exp(highest - peak)
    own_factor = jnp.exp(own - peak)
    numer = sums * cache_factor[..., None] + value_heads * own_factor[..., None]
    denom = totals * cache_factor + own_factor
    attention = (
        (numer / denom[..., None]).astype(jnp.bfloat16).reshape(batch_rows, local_heads * head_size)
    )
    partial_value = jnp.dot(attention, out_weight, preferred_element_type=jnp.float32)
    piece_width = stream.shape[1]
    block_width = partial_value.shape[1]
    block_sum = lax.psum(partial_value, "tp")
    own_block = lax.dynamic_slice_in_dim(
        gathered, lax.axis_index("kv") * block_width, block_width, 1
    )
    middle_block = (own_block.astype(jnp.float32) + block_sum).astype(jnp.bfloat16)
    squares = lax.psum(row_squares(middle_block), "kv")
    middle_piece = lax.dynamic_slice_in_dim(
        middle_block, lax.axis_index("tp") * piece_width, piece_width, 1
    )
    inverse = lax.rsqrt(squares / D + EPS)
    gain_block = lax.dynamic_slice_in_dim(
        channel_gain, lax.axis_index("kv") * block_width, block_width, 0
    )
    mixed_block = (
        middle_block.astype(jnp.float32) * inverse[:, None] * gain_block[None, :]
    ).astype(jnp.bfloat16)
    up_partial = jnp.dot(mixed_block, up_weight, preferred_element_type=jnp.float32)
    hidden = squared_relu(lax.psum(up_partial, "kv"))
    down_partial = jnp.dot(hidden, down_weight, preferred_element_type=jnp.float32)
    reduced = lax.psum_scatter(down_partial, "tp", scatter_dimension=1, tiled=True)
    return (middle_piece.astype(jnp.float32) + reduced).astype(jnp.bfloat16)


def solution(mesh):
    return jax.shard_map(
        shards,
        mesh=mesh,
        in_specs=(
            P(None, ("kv", "tp")),
            P(),
            P(None, "tp"),
            P(None, "tp"),
            P(None, "tp"),
            P(),
            P(),
            P(None, "tp", "kv", None),
            P(None, "tp", "kv", None),
            P(None, "tp", "kv"),
            P("tp", "kv"),
            P(),
            P("kv", "tp"),
            P("tp", "kv"),
        ),
        out_specs=P(None, ("kv", "tp")),
        check_vma=False,
    )
```

profile of v0, /device:TPU:0, one launch (start us, length us, event | category | flops | bytes accessed | tf_op | source)
XLA Modules:
  0.0 247.9 jit_solution(13276194251928122677)
XLA Ops:
  6.5 44.6 %all_gather.21 = bf16[32,4096]{1,0:T(8,128)(2,1)S(1)} all-gather(bf16[32,128]{1,0:T(8,128)(2,1)} %param.16), channel_id=1, replica_groups=mesh['kv'=4,'tp'=8] {'kv','tp'}, dimensions={1}, use_global_device_ids=true | all-gather | bytes 270336 | tf_op jit(solution)/shard_map/all_gather | solution.py:69
  51.4 1.0 convolution_convert_fusion.2
  52.6 1.2 fusion.40
  53.9 4.6 %fusion.41 = f32[32,2,1,1024]{3,2,1,0:T(1,128)S(1)} fusion(bf16[32,2,64,1]{2,3,1,0:T(2,128)(2,1)S(1)} %reshape.57, bf16[32,2,1024,64]{2,3,1,0:T(8,128)(2,1)} %param.23), kind=kOutput, calls=%fused_computation.63 | convolution fusion | flops 8388608 | bytes 8658944 | tf_op jit(solution)/shard_map/bhd,bhpd->bhp/dot_general | solution.py:84
  58.5 2.1 fusion.38
  60.6 1.3 fusion.30
  61.9 5.7 %fusion.11 = f32[32,2,1,64]{3,2,1,0:T(1,128)S(1)} fusion(bf16[32,2,1024,64]{2,3,1,0:T(8,128)(2,1)} %param.24, bf16[32,2,1024,1]{2,1,0,3:T(2,128)(2,1)S(1)} %get-tuple-element.211), kind=kOutput, calls=%fused_computation.24 | convolution fusion | flops 8388608 | bytes 8536064 | tf_op jit(solution)/shard_map/bhp,bhpd->bhd/dot_general | solution.py:92
  67.6 7.5 %all-gather.2 = f32[128,2,64]{2,1,0:T(2,128)S(1)} all-gather(f32[32,2,64]{2,1,0:T(2,128)S(1)} %bitcast.49), channel_id=4, replica_groups=mesh['kv'=4,'tp'=8] {'kv'}, dimensions={0}, use_global_device_ids=true | all-gather | bytes 81920 | tf_op jit(solution)/shard_map/all_gather | solution.py:11
  75.8 8.1 %all-gather.4 = f32[4,32,2]{1,2,0:T(2,128)S(1)} all-gather(f32[1,32,2]{1,2,0:T(2,128)S(1)} %bitcast.51), channel_id=3, replica_groups=mesh['kv'=4,'tp'=8] {'kv'}, dimensions={0}, use_global_device_ids=true | all-gather | bytes 1280 | tf_op jit(solution)/shard_map/all_gather | solution.py:11
  83.8 7.1 %all-gather.3 = f32[4,32,2]{1,2,0:T(2,128)S(1)} all-gather(f32[1,32,2]{1,2,0:T(2,128)S(1)} %bitcast.50), channel_id=2, replica_groups=mesh['kv'=4,'tp'=8] {'kv'}, dimensions={0}, use_global_device_ids=true | all-gather | bytes 1280 | tf_op jit(solution)/shard_map/all_gather | solution.py:11
  90.9 3.6 %while.19 = (s32[]{:T(128)}, f32[32,2]{0,1:T(2,128)S(1)}, f32[32,2]{0,1:T(2,128)S(1)}, f32[32,2,64]{2,1,0:T(2,128)S(1)}, f32[4,32,2]{1,2,0:T(2,128)S(1)}, /*inde...) while((s32[]{:T(128)}, f32[32,2]{0,1:T(2,128)S(1)}, ...), condition=%wide.region_4.5_spmd, body=%wide.region_3.4_spmd.sunk | while | flops 12677 | bytes 52887 | solution.py:16
  91.1 1.0 fusion.57
  92.3 1.0 fusion.57
  93.5 1.0 fusion.57
  96.2 1.8 fusion.42
  98.0 0.7 dynamic_slice.59
  98.7 51.7 %all-reduce.3.cloned.1.call-done = f32[32,1024]{1,0:T(8,128)} async-done(((f32[32,1024]{1,0:T(8,128)}), f32[32,1024]{1,0:T(8,128)}) %all-reduce.3.cloned.1.call-update) | async-done | bytes 131088 | tf_op jit(solution)/shard_map/psum | solution.py:108
  150.4 1.0 fusion.13
  151.4 9.8 %psum.22 = f32[32]{0:T(128)S(1)} all-reduce(f32[32]{0:T(128)S(1)} %get-tuple-element.204), channel_id=1, replica_groups=mesh['kv'=4,'tp'=8] {'kv'}, use_global_device_ids=true, to_apply=%region_8.9 | all-reduce | flops 32 | bytes 256 | tf_op jit(solution)/shard_map/psum | solution.py:113
  161.3 3.8 %fusion.18 = f32[32,2048]{1,0:T(8,128)} fusion(bf16[1024,2048]{1,0:T(8,128)(2,1)} %param.28, bf16[32,1024]{1,0:T(8,128)(2,1)S(1)} %get-tuple-element.205, f32[1024]{0:T(1024)S(1)} %dynamic_slice.59, f32[32]{0:T(128)S(1)} %add_rsqrt_fusion), kind=kOutput, calls=%fused_computation.37 | convolution fusion | flops 134348800 | bytes 4526208 | tf_op jit(solution)/shard_map/dot_general | solution.py:124
  165.1 40.4 %all-reduce.5.cloned.1.call-done = f32[32,2048]{1,0:T(8,128)} async-done(((f32[32,2048]{1,0:T(8,128)}), f32[32,2048]{1,0:T(8,128)}) %all-reduce.5.cloned.1.call-update) | async-done | bytes 262160 | tf_op jit(solution)/shard_map/psum | solution.py:125
  205.5 3.8 %fusion.16 = f32[32,1024]{1,0:T(8,128)} fusion(bf16[2048,1024]{1,0:T(8,128)(2,1)} %param.29, f32[32,2048]{1,0:T(8,128)} %all-reduce.5.cloned.1.call-done), kind=kOutput, calls=%fused_computation.34 | convolution fusion | flops 134414336 | bytes 4587520 | tf_op jit(solution)/shard_map/dot_general | solution.py:126
  209.3 30.7 %reduce-scatter.2.cloned.1.call-done = f32[32,128]{1,0:T(8,128)} async-done(((f32[32,1024]{1,0:T(8,128)}), f32[32,128]{1,0:T(8,128)}) %reduce-scatter.2.cloned.1.call-update) | async-done | bytes 16400 | tf_op jit(solution)/shard_map/reduce_scatter | solution.py:127
  240.0 1.3 add_convert_fusion.1
  (49 shorter events, 3.6 us)
Async XLA Ops:
  6.5 44.8 %copy-start = (bf16[4096,128]{1,0:T(8,128)(2,1)S(1)}, bf16[4096,128]{1,0:T(8,128)(2,1)}, u32[]{:S(2)}) copy-start(bf16[4096,128]{1,0:T(8,128)(2,1)} %param.18) | copy-start | bytes 3145732
  6.5 143.8 %all-reduce.3.cloned.1.call-start = ((), (), s32[]{:S(2)}) async-start(), calls=%async_computation.1 | async-start | bytes 262144 | tf_op jit(solution)/shard_map/psum | solution.py:108
  58.4 36.1 %copy-start.1 = (bf16[4096,128]{1,0:T(8,128)(2,1)S(1)}, bf16[4096,128]{1,0:T(8,128)(2,1)}, u32[]{:S(2)}) copy-start(bf16[4096,128]{1,0:T(8,128)(2,1)} %param.19) | copy-start | bytes 3145732
  58.4 36.1 %copy-start.4 = (f32[4096]{0:T(1024)S(1)}, f32[4096]{0:T(1024)}, u32[]{:S(2)}) copy-start(f32[4096]{0:T(1024)} %param.17) | copy-start | bytes 49156
  58.5 37.0 %copy-start.2 = (bf16[4096,128]{1,0:T(8,128)(2,1)S(1)}, bf16[4096,128]{1,0:T(8,128)(2,1)}, u32[]{:S(2)}) copy-start(bf16[4096,128]{1,0:T(8,128)(2,1)} %param.20) | copy-start | bytes 3145732
  75.0 0.6 copy-start.3
  98.0 107.5 %all-reduce.5.cloned.1.call-start = ((), (), s32[]{:S(2)}) async-start(), calls=%async_computation.2 | async-start | bytes 524288 | tf_op jit(solution)/shard_map/psum | solution.py:125
  165.1 75.0 %reduce-scatter.2.cloned.1.call-start = ((), (), s32[]{:S(2)}) async-start(), calls=%async_computation.3 | async-start | bytes 147456 | tf_op jit(solution)/shard_map/reduce_scatter | solution.py:127
Sparse Core Ops, SparseCore 0:
  98.1 52.2 all-reduce.2
  165.2 40.2 all-reduce.4
  209.4 30.5 reduce-scatter.1
where the time goes:
time: 249 us; the launch traced here: 248 us
  waiting for transfers between devices  123 us (49%)
  blocking collectives  77.1 us (31%)
  matrix products  22.4 us (9%)
  between operations  13.2 us (5%)
  other arithmetic  9.28 us (4%)
  local copies, waits for them, and re-layouts  2.9 us (1%)
    psum x1, waiting for transfers between devices, shards(): block_sum = lax.psum(partial_value, 'tp')  51.7 us
    all_gather x1, blocking collectives, shards(): gathered = lax.all_gather(stream, ('kv', 'tp'), axis=1, tiled=True)  44.6 us
    psum x1, waiting for transfers between devices, shards(): hidden = squared_relu(lax.psum(up_partial, 'kv'))  40.4 us
    reduce_scatter x1, waiting for transfers between devices, shards(): lax.psum_scatter(down_partial, 'tp', scatter_dimension=1, tiled=True)  30.7 us
    all_gather x3, blocking collectives, combined_all(): gathered = jax.tree.map(lambda a: lax.all_gather(a, axis), part)  22.6 us
    psum x1, blocking collectives, shards(): squares = lax.psum(row_squares(middle_block), 'kv')  9.84 us
    dot_general x1, matrix products, shards(): jnp.einsum('bhp,bhpd->bhd', weights, value_cache, preferred_element_type=...  5.65 us
  transfers between devices with their start and end apart: 3, of which 3 were waited for; matrix products, arithmetic and copies ran while one was open for 0% of the time, Pallas kernels for 0%

commit v1 on v0

--- a/solution.py
+++ b/solution.py
@@ -5,6 +5,10 @@
 
 D = 4096
 EPS = 1e-06
+
+
+def _step_on_cards(my_tile, link_axis):
+    return jnp.sum(jax.lax.all_gather(my_tile, axis_name=link_axis), 0)
 
 
 def combined_all(part, axis, combine):
@@ -105,7 +109,7 @@
     partial_value = jnp.dot(attention, out_weight, preferred_element_type=jnp.float32)
     piece_width = stream.shape[1]
     block_width = partial_value.shape[1]
-    block_sum = lax.psum(partial_value, "tp")
+    block_sum = _step_on_cards(partial_value, link_axis="tp")
     own_block = lax.dynamic_slice_in_dim(
         gathered, lax.axis_index("kv") * block_width, block_width, 1
     )

time: 249 us -> 217 us (0.87)
  waiting for transfers between devices: 123 us -> 90.7 us
    psum x1 -> x0, waiting for transfers between devices: 51.7 us -> none  [shards(): block_sum = lax.psum(partial_value, 'tp')]
    all_gather x0 -> x1, waiting for transfers between devices: none -> 18.9 us  [_step_on_cards(): return jnp.sum(jax.lax.all_gather(my_tile, axis_name=link_axis), 0)]
where the time goes in v1:
time: 217 us; the launch traced here: 216 us
  waiting for transfers between devices  90.7 us (42%)
  blocking collectives  77.1 us (36%)
  matrix products  22.4 us (10%)
  between operations  13.2 us (6%)
  other arithmetic  9.68 us (4%)
  local copies, waits for them, and re-layouts  2.9 us (1%)
    all_gather x1, blocking collectives, shards(): gathered = lax.all_gather(stream, ('kv', 'tp'), axis=1, tiled=True)  44.6 us
    psum x1, waiting for transfers between devices, shards(): hidden = squared_relu(lax.psum(up_partial, 'kv'))  40.9 us
    reduce_scatter x1, waiting for transfers between devices, shards(): lax.psum_scatter(down_partial, 'tp', scatter_dimension=1, tiled=True)  30.7 us
    all_gather x3, blocking collectives, combined_all(): gathered = jax.tree.map(lambda a: lax.all_gather(a, axis), part)  22.6 us
    all_gather x1, waiting for transfers between devices, _step_on_cards(): return jnp.sum(jax.lax.all_gather(my_tile, axis_name=link_axis), 0)  18.9 us
    psum x1, blocking collectives, shards(): squares = lax.psum(row_squares(middle_block), 'kv')  9.83 us
    dot_general x1, matrix products, shards(): jnp.einsum('bhp,bhpd->bhd', weights, value_cache, preferred_element_type=...  5.65 us
    dot_general x1, matrix products, shards(): jnp.einsum('bhd,bhpd->bhp', query_heads, key_cache, preferred_element_typ...  4.59 us
  transfers between devices with their start and end apart: 3, of which 3 were waited for; matrix products, arithmetic and copies ran while one was open for 0% of the time, Pallas kernels for 0%

profile of v1, /device:TPU:0, one launch (start us, length us, event | category | flops | bytes accessed | tf_op | source)
XLA Modules:
  0.0 216.1 jit_solution(4532986432456008099)
XLA Ops:
  6.5 44.6 %all_gather.27 = bf16[32,4096]{1,0:T(8,128)(2,1)S(1)} all-gather(bf16[32,128]{1,0:T(8,128)(2,1)} %param.16), channel_id=1, replica_groups=mesh['kv'=4,'tp'=8] {'kv','tp'}, dimensions={1}, use_global_device_ids=true | all-gather | bytes 270336 | tf_op jit(solution)/shard_map/all_gather | solution.py:73
  51.4 1.0 convolution_convert_fusion.2
  52.6 1.2 fusion.40
  53.9 4.6 %fusion.41 = f32[32,2,1,1024]{3,2,1,0:T(1,128)S(1)} fusion(bf16[32,2,64,1]{2,3,1,0:T(2,128)(2,1)S(1)} %reshape.58, bf16[32,2,1024,64]{2,3,1,0:T(8,128)(2,1)} %param.23), kind=kOutput, calls=%fused_computation.63 | convolution fusion | flops 8388608 | bytes 8658944 | tf_op jit(solution)/shard_map/bhd,bhpd->bhp/dot_general | solution.py:88
  58.5 2.1 fusion.38
  60.6 1.3 fusion.30
  61.9 5.7 %fusion.11 = f32[32,2,1,64]{3,2,1,0:T(1,128)S(1)} fusion(bf16[32,2,1024,64]{2,3,1,0:T(8,128)(2,1)} %param.24, bf16[32,2,1024,1]{2,1,0,3:T(2,128)(2,1)S(1)} %get-tuple-element.211), kind=kOutput, calls=%fused_computation.24 | convolution fusion | flops 8388608 | bytes 8536064 | tf_op jit(solution)/shard_map/bhp,bhpd->bhd/dot_general | solution.py:96
  67.6 7.5 %all-gather.2 = f32[128,2,64]{2,1,0:T(2,128)S(1)} all-gather(f32[32,2,64]{2,1,0:T(2,128)S(1)} %bitcast.51), channel_id=4, replica_groups=mesh['kv'=4,'tp'=8] {'kv'}, dimensions={0}, use_global_device_ids=true | all-gather | bytes 81920 | tf_op jit(solution)/shard_map/all_gather | solution.py:15
  75.8 8.1 %all-gather.5 = f32[4,32,2]{1,2,0:T(2,128)S(1)} all-gather(f32[1,32,2]{1,2,0:T(2,128)S(1)} %bitcast.53), channel_id=3, replica_groups=mesh['kv'=4,'tp'=8] {'kv'}, dimensions={0}, use_global_device_ids=true | all-gather | bytes 1280 | tf_op jit(solution)/shard_map/all_gather | solution.py:15
  83.8 7.1 %all-gather.4 = f32[4,32,2]{1,2,0:T(2,128)S(1)} all-gather(f32[1,32,2]{1,2,0:T(2,128)S(1)} %bitcast.52), channel_id=2, replica_groups=mesh['kv'=4,'tp'=8] {'kv'}, dimensions={0}, use_global_device_ids=true | all-gather | bytes 1280 | tf_op jit(solution)/shard_map/all_gather | solution.py:15
  90.9 3.6 %while.19 = (s32[]{:T(128)}, f32[32,2]{0,1:T(2,128)S(1)}, f32[32,2]{0,1:T(2,128)S(1)}, f32[32,2,64]{2,1,0:T(2,128)S(1)}, f32[4,32,2]{1,2,0:T(2,128)S(1)}, /*inde...) while((s32[]{:T(128)}, f32[32,2]{0,1:T(2,128)S(1)}, ...), condition=%wide.region_4.5_spmd, body=%wide.region_3.4_spmd.sunk | while | flops 12677 | bytes 52887 | solution.py:20
  91.1 1.0 fusion.57
  92.3 1.0 fusion.57
  93.5 1.0 fusion.57
  96.2 1.8 fusion.42
  98.0 0.7 dynamic_slice.59
  98.7 18.9 %all-gather.8.cloned.1.call-done = f32[256,1024]{1,0:T(8,128)} async-done(((f32[32,1024]{1,0:T(8,128)}), f32[256,1024]{1,0:T(8,128)}) %all-gather.8.cloned.1.call-update) | async-done | bytes 1048592 | tf_op jit(solution)/shard_map/all_gather | solution.py:11
  117.6 1.3 reduce_sum.48
  119.1 9.8 %psum.14 = f32[32]{0:T(128)S(1)} all-reduce(f32[32]{0:T(128)S(1)} %get-tuple-element.204), channel_id=1, replica_groups=mesh['kv'=4,'tp'=8] {'kv'}, use_global_device_ids=true, to_apply=%region_8.9 | all-reduce | flops 32 | bytes 256 | tf_op jit(solution)/shard_map/psum | solution.py:117
  128.9 3.8 %fusion.18 = f32[32,2048]{1,0:T(8,128)} fusion(bf16[1024,2048]{1,0:T(8,128)(2,1)} %param.28, bf16[32,1024]{1,0:T(8,128)(2,1)S(1)} %get-tuple-element.205, f32[1024]{0:T(1024)S(1)} %dynamic_slice.59, f32[32]{0:T(128)S(1)} %add_rsqrt_fusion), kind=kOutput, calls=%fused_computation.37 | convolution fusion | flops 134348800 | bytes 4526208 | tf_op jit(solution)/shard_map/dot_general | solution.py:128
  132.8 40.9 %all-reduce.2.cloned.1.call-done = f32[32,2048]{1,0:T(8,128)} async-done(((f32[32,2048]{1,0:T(8,128)}), f32[32,2048]{1,0:T(8,128)}) %all-reduce.2.cloned.1.call-update) | async-done | bytes 262160 | tf_op jit(solution)/shard_map/psum | solution.py:129
  173.7 3.8 %fusion.16 = f32[32,1024]{1,0:T(8,128)} fusion(bf16[2048,1024]{1,0:T(8,128)(2,1)} %param.29, f32[32,2048]{1,0:T(8,128)} %all-reduce.2.cloned.1.call-done), kind=kOutput, calls=%fused_computation.34 | convolution fusion | flops 134414336 | bytes 4587520 | tf_op jit(solution)/shard_map/dot_general | solution.py:130
  177.5 30.7 %reduce-scatter.2.cloned.1.call-done = f32[32,128]{1,0:T(8,128)} async-done(((f32[32,1024]{1,0:T(8,128)}), f32[32,128]{1,0:T(8,128)}) %reduce-scatter.2.cloned.1.call-update) | async-done | bytes 16400 | tf_op jit(solution)/shard_map/reduce_scatter | solution.py:131
  208.2 1.3 add_convert_fusion.1
  (50 shorter events, 3.7 us)
Async XLA Ops:
  6.5 44.8 %copy-start = (bf16[4096,128]{1,0:T(8,128)(2,1)S(1)}, bf16[4096,128]{1,0:T(8,128)(2,1)}, u32[]{:S(2)}) copy-start(bf16[4096,128]{1,0:T(8,128)(2,1)} %param.18) | copy-start | bytes 3145732
  6.5 111.1 %all-gather.8.cloned.1.call-start = ((), (), s32[]{:S(2)}) async-start(), calls=%async_computation.3 | async-start | bytes 1179648 | tf_op jit(solution)/shard_map/all_gather | solution.py:11
  58.4 36.1 %copy-start.1 = (bf16[4096,128]{1,0:T(8,128)(2,1)S(1)}, bf16[4096,128]{1,0:T(8,128)(2,1)}, u32[]{:S(2)}) copy-start(bf16[4096,128]{1,0:T(8,128)(2,1)} %param.19) | copy-start | bytes 3145732
  58.4 36.1 %copy-start.4 = (f32[4096]{0:T(1024)S(1)}, f32[4096]{0:T(1024)}, u32[]{:S(2)}) copy-start(f32[4096]{0:T(1024)} %param.17) | copy-start | bytes 49156
  58.5 37.0 %copy-start.2 = (bf16[4096,128]{1,0:T(8,128)(2,1)S(1)}, bf16[4096,128]{1,0:T(8,128)(2,1)}, u32[]{:S(2)}) copy-start(bf16[4096,128]{1,0:T(8,128)(2,1)} %param.20) | copy-start | bytes 3145732
  75.0 0.6 copy-start.3
  98.0 75.7 %all-reduce.2.cloned.1.call-start = ((), (), s32[]{:S(2)}) async-start(), calls=%async_computation.1 | async-start | bytes 524288 | tf_op jit(solution)/shard_map/psum | solution.py:129
  132.7 75.5 %reduce-scatter.2.cloned.1.call-start = ((), (), s32[]{:S(2)}) async-start(), calls=%async_computation.2 | async-start | bytes 147456 | tf_op jit(solution)/shard_map/reduce_scatter | solution.py:131
Sparse Core Ops, SparseCore 0:
  98.1 19.5 all-gather.7
  132.8 40.8 all-reduce.1
  177.6 30.5 reduce-scatter.1
